TPU v7x, 512 devices: a whole 4x8x8 slice. The times are simulated.
512 devices in a mesh: sp: 64 (over z, y), fs: 4 (over x), tp: 2 (over core).
Axes of the slice: x: 4, y: 8, z: 8, core: 2. Of those that a mesh axis runs over, the one named last changes fastest.
Arguments:
- tokens: bfloat16 [32768, 2048], P(('fs', 'sp')), parts along dimension 0, may hold values from -6 to 6
- norm_gain: bfloat16 [2048], replicated, may hold values from 0.099609375 to 1.8984375
- query_down: bfloat16 [2048, 512], P('sp'), may hold values from -0.125 to 0.125
- query_gain: bfloat16 [512], replicated, may hold values from 0.099609375 to 1.8984375
- latent_down: bfloat16 [2048, 256], replicated, may hold values from -0.125 to 0.125
- latent_gain: bfloat16 [256], replicated, may hold values from 0.099609375 to 1.8984375
- rope_down: bfloat16 [2048, 64], replicated, may hold values from -30 to 30
- query_up: bfloat16 [512, 1536], P(None, 'tp'), may hold values from -0.25 to 0.25
- key_up: bfloat16 [256, 1024], P(None, 'tp'), may hold values from -0.75 to 0.75
- value_up: bfloat16 [256, 1024], P(None, 'tp'), may hold values from -0.375 to 0.375
- glu_value: bfloat16 [2048, 1024], P('sp', 'tp'), may hold values from -0.125 to 0.125
- glu_gate: bfloat16 [2048, 1024], P('sp', 'tp'), may hold values from -0.125 to 0.125
- conv_taps: bfloat16 [31, 1024], P(None, 'tp'), may hold values from -1 to 1
- group_gain: bfloat16 [1024], P('tp'), may hold values from 0.099609375 to 1.8984375
- head_proj: bfloat16 [1024, 2048], P('tp', 'sp'), may hold values from -0.75 to 0.75
- channel_proj: bfloat16 [1024, 2048], P('tp', 'sp'), may hold values from -0.1875 to 0.1875
Outputs:
- mixed_out: bfloat16 [32768, 2048], P(('fs', 'sp'), 'tp'), parts along dimension 0
- log_weight: float32 [8, 32768], P('tp', ('fs', 'sp')), parts along dimension 1
There are 4 independent parts, one for each index of `fs`. A program takes and returns all parts, laid end to end along the dimension named above; an argument that names none is the same for every part. Nothing has to cross between parts.
All inputs are finite; a program needn't handle non-finite values.
Results may differ from a plain program's by a relative error of at most 0.015.
The roundings to bfloat16 on the way count: a program that leaves them out, or rounds other values in their place, can miss the bound.
Values may be sent and summed in bfloat16 or wider, within the bound.
No kernel may reach another device: no remote copies, remote signals or barrier semaphores. Data moves between devices by JAX's collectives and lax.ppermute only.
A program may use at most 128 MiB of HBM per device.

v0:
```python
import jax
import jax.numpy as jnp
from jax import lax
from jax.sharding import PartitionSpec as P

NOPE = 128
ROPE = 64
VDIM = 128
KVR = 256
CH = 1024
GROUPS = 8
GRID_W = 64
norm_eps = 1e-06
rope_base = 10000.0
far_below = -1e30


def in_one_piece(arrays, axis, dim, along):
    widths = [a.shape[along] for a in arrays]
    both = jnp.concatenate(arrays, axis=along)
    result = lax.all_gather(both, axis, axis=dim, tiled=True)
    return tuple(jnp.split(result, [sum(widths[:k]) for k in range(1, len(widths))], axis=along))


def padded_2(block, sides, width):
    for axis, dim in sides:
        count = lax.axis_size(axis)
        forward = [(i, i + 1) for i in range(count - 1)]
        backward = [(target, source) for source, target in forward]
        low = lax.ppermute(
            lax.slice_in_dim(block, block.shape[dim] - width, None, axis=dim), axis, forward
        )
        high = lax.ppermute(lax.slice_in_dim(block, 0, width, axis=dim), axis, backward)
        block = jnp.concatenate([low, block, high], axis=dim)
    return block


def split_up(shard, dim, length):
    before, after = (shard.shape[:dim], shard.shape[dim + 1 :])
    return jnp.moveaxis(shard.reshape(*before, length, -1, *after), dim, 0)


def sent_and_summed(shard, axis, dim):
    tiles = split_up(shard, dim, lax.axis_size(axis))
    arrived = lax.all_to_all(tiles, axis, split_axis=0, concat_axis=0, tiled=True)
    return arrived.astype(jnp.float32).sum(axis=0)


def rms_scale(values, scale_gain):
    inv_rms = lax.rsqrt(jnp.mean(values * values, axis=-1, keepdims=True) + norm_eps)
    return values * inv_rms * scale_gain.astype(jnp.float32)


def angles_for(positions, rope_size):
    quarter = rope_size // 4
    inverse = rope_base ** (-jnp.arange(quarter, dtype=jnp.float32) / quarter)
    grid_row = (positions // GRID_W).astype(jnp.float32)
    grid_col = (positions % GRID_W).astype(jnp.float32)
    return jnp.concatenate([grid_row[:, None] * inverse, grid_col[:, None] * inverse], axis=-1)


def rotate(values, angles):
    half_size = values.shape[-1] // 2
    front_half = values[..., :half_size]
    back_half = values[..., half_size:]
    cosine = jnp.cos(angles)
    sine_part = jnp.sin(angles)
    return jnp.concatenate(
        [front_half * cosine - back_half * sine_part, back_half * cosine + front_half * sine_part],
        axis=-1,
    )


def key_block(normed, latent_down, latent_gain, rope_down, positions):
    latent = jnp.dot(normed, latent_down, preferred_element_type=jnp.float32)
    latent = rms_scale(latent, latent_gain).astype(jnp.bfloat16)
    rope_key = jnp.dot(normed, rope_down, preferred_element_type=jnp.float32)
    rope_key = rotate(rope_key, angles_for(positions, rope_key.shape[-1])).astype(jnp.bfloat16)
    return jnp.concatenate([latent, rope_key], axis=1)


def per_device(
    tokens,
    norm_gain,
    query_down,
    query_gain,
    latent_down,
    latent_gain,
    rope_down,
    query_up,
    key_up,
    value_up,
    glu_value,
    glu_gate,
    conv_taps,
    group_gain,
    head_proj,
    channel_proj,
):
    tok_count = tokens.shape[0]
    reach_rows = conv_taps.shape[0] // 2
    head_count = key_up.shape[1] // NOPE
    normed = rms_scale(tokens.astype(jnp.float32), norm_gain).astype(jnp.bfloat16)
    offsets = lax.axis_index("sp") * tok_count + jnp.arange(tok_count, dtype=jnp.int32)
    blocks = in_one_piece((query_down, glu_value, glu_gate), "sp", 0, 1)
    query_latent = jnp.dot(normed, blocks[0], preferred_element_type=jnp.float32)
    value_in = jnp.dot(normed, blocks[1], preferred_element_type=jnp.float32)
    gate_in = jnp.dot(normed, blocks[2], preferred_element_type=jnp.float32)
    latent_query = rms_scale(query_latent, query_gain).astype(jnp.bfloat16)
    query_all = jnp.dot(latent_query, query_up, preferred_element_type=jnp.float32).reshape(
        tok_count, head_count, NOPE + ROPE
    )
    query_plain = query_all[:, :, :NOPE].astype(jnp.bfloat16)
    query_rope = rotate(query_all[:, :, NOPE:], angles_for(offsets, ROPE)[:, None, :]).astype(
        jnp.bfloat16
    )
    absorbed = jnp.einsum(
        "thd,rhd->htr",
        query_plain,
        key_up.reshape(KVR, head_count, NOPE),
        preferred_element_type=jnp.float32,
    ).astype(jnp.bfloat16)
    queries = jnp.concatenate([absorbed, jnp.transpose(query_rope, (1, 0, 2))], axis=-1)
    score_scale = (NOPE + ROPE) ** (-0.5)
    half_rows = tok_count // lax.axis_size("tp")
    first_row = lax.axis_index("tp") * half_rows
    own_rows = lax.dynamic_slice_in_dim(normed, first_row, half_rows, 0)
    own_positions = lax.dynamic_slice_in_dim(offsets, first_row, half_rows, 0)
    own_keys = key_block(own_rows, latent_down, latent_gain, rope_down, own_positions)
    block_keys = lax.all_gather(own_keys, ("sp", "tp"), axis=0, tiled=True)
    row_max = jnp.full((head_count, tok_count), far_below, jnp.float32)
    scores = (
        jnp.einsum("hqc,kc->hqk", queries, block_keys, preferred_element_type=jnp.float32)
        * score_scale
    )
    new_max = jnp.maximum(row_max, jnp.max(scores, axis=2))
    weights = jnp.exp(scores - new_max[:, :, None])
    new_sum = jnp.sum(weights, axis=2)
    added = jnp.einsum(
        "hqk,kr->hqr",
        weights.astype(jnp.bfloat16),
        block_keys[:, :KVR],
        preferred_element_type=jnp.float32,
    )
    gated_rows = (value_in * jax.nn.sigmoid(gate_in)).astype(jnp.bfloat16)
    padded = padded_2(gated_rows, (("sp", 0),), reach_rows)
    filtered = padded[0:tok_count].astype(jnp.float32) * conv_taps[0].astype(jnp.float32)
    for tap_index in range(1, conv_taps.shape[0]):
        filtered = filtered + padded[tap_index : tap_index + tok_count].astype(
            jnp.float32
        ) * conv_taps[tap_index].astype(jnp.float32)
    grouped = filtered.reshape(tok_count, -1, CH // GROUPS)
    centred = grouped - jnp.mean(grouped, axis=-1, keepdims=True)
    spread = jnp.mean(centred * centred, axis=-1, keepdims=True)
    normal_groups = (centred * lax.rsqrt(spread + norm_eps)).reshape(tok_count, -1)
    conv_branch = jax.nn.silu(normal_groups * group_gain.astype(jnp.float32)).astype(jnp.bfloat16)
    attended = (added / new_sum[:, :, None]).astype(jnp.bfloat16)
    log_weight = new_max + jnp.log(new_sum)
    head_out = jnp.einsum(
        "htr,rhv->thv",
        attended,
        value_up.reshape(KVR, head_count, VDIM),
        preferred_element_type=jnp.float32,
    )
    head_out = head_out.reshape(tok_count, head_count * VDIM).astype(jnp.bfloat16)
    mixed_in = jnp.concatenate([head_out, conv_branch], axis=1)
    out_weight = jnp.concatenate([head_proj, channel_proj], axis=0)
    partial_terms = jnp.dot(
        mixed_in,
        lax.all_gather(out_weight, "sp", axis=1, tiled=True),
        preferred_element_type=jnp.float32,
    )
    mixed_out = sent_and_summed(partial_terms.astype(jnp.bfloat16), "tp", 1).astype(jnp.bfloat16)
    return (mixed_out, log_weight)


def solution(mesh):
    in_specs = (
        P(("fs", "sp"), None),
        P(),
        P("sp", None),
        P(),
        P(),
        P(),
        P(),
        P(None, "tp"),
        P(None, "tp"),
        P(None, "tp"),
        P("sp", "tp"),
        P("sp", "tp"),
        P(None, "tp"),
        P("tp"),
        P("tp", "sp"),
        P("tp", "sp"),
    )
    out_specs = (P(("fs", "sp"), "tp"), P("tp", ("fs", "sp")))
    return jax.shard_map(
        per_device, mesh=mesh, in_specs=in_specs, out_specs=out_specs, check_vma=False
    )
```

profile of v0, /device:TPU:1, one launch (start us, length us, event | category | flops | bytes accessed | tf_op | source)
XLA Modules:
  0.0 295.6 jit_solution(11499413010207656620)
XLA Ops:
  7.2 1.5 pad_maximum_fusion.2
  8.8 0.7 convert_element_type.239
  9.5 0.7 convert_element_type.232
  10.3 1.2 fusion.32
  11.5 1.2 fusion.34
  12.8 0.4 multiply_reduce_fusion.3
  13.3 1.2 fusion.53
  14.7 0.7 pad_maximum_fusion.4
  15.5 1.4 pad_maximum_fusion.3
  17.0 0.7 convert_element_type.234
  17.7 0.7 convert_element_type.280
  18.7 1.1 copy.70
  19.8 1.0 slice_convert_fusion.31
  20.8 1.0 slice_convert_fusion.32
  21.8 84.6 %all-gather.4.cloned.1.call-done = bf16[2048,1536]{1,0:T(8,128)(2,1)} async-done(((bf16[32,1536]{1,0:T(8,128)(2,1)}), bf16[2048,1536]{1,0:T(8,128)(2,1)}) %all-gather.4.cloned.1.call-update) | async-done | bytes 6291472 | tf_op jit(solution)/shard_map/all_gather | solution.py:21
  106.4 2.1 fusion.26
  108.5 2.1 fusion.29
  110.6 1.9 collective-permute-start
  112.6 1.3 collective-permute-start.1
  113.9 2.1 multiply_reduce_fusion.2
  116.0 0.5 fusion.57
  117.3 76.4 %all-gather.6.cloned.1.call-done = bf16[8192,320]{1,0:T(8,128)(2,1)} async-done(((bf16[64,320]{1,0:T(8,128)(2,1)}), bf16[8192,320]{1,0:T(8,128)(2,1)}) %all-gather.6.cloned.1.call-update) | async-done | bytes 5242896 | tf_op jit(solution)/shard_map/all_gather | solution.py:130
  193.6 10.9 %multiply_reduce_fusion = (f32[4,128]{1,0:T(4,128)S(1)}, f32[4,128,8192]{2,1,0:T(8,128)}) fusion(bf16[8192,320]{1,0:T(8,128)(2,1)} %all-gather.6.cloned.1.call-done, bf16[4,128,64]{2,1,0:T(8,128)(2,1)S(1)} %maximum_bitcast_fusion, bf16[4,128,256]{2,1,0:T(8,128)(2,1)S(1)} %convolution_convert_fusion.1), kind=kOutput, calls=%fused_computation.1 | convolution fusion | flops 2693398016 | bytes 22349824 | tf_op jit(solution)/shard_map/hqc,kc->hqk/dot_general | solution.py:133
  204.5 8.7 %fusion = f32[4,128]{1,0:T(4,128)S(1)} fusion(f32[4,128,8192]{2,1,0:T(8,128)} %get-tuple-element.54, f32[4,128]{1,0:T(4,128)S(1)} %broadcast_maximum_fusion), kind=kLoop, calls=%fused_computation.2 | loop fusion | flops 12582400 | bytes 16781312 | tf_op jit(solution)/shard_map/reduce_sum | solution.py:138
  213.2 9.9 %convolution_convert_fusion.2 = bf16[4,128,128]{1,2,0:T(8,128)(2,1)S(1)} fusion(bf16[256,4,128]{0,2,1:T(8,128)(2,1)S(1)} %bitcast.94, bf16[8192,320]{1,0:T(8,128)(2,1)} %all-gather.6.cloned.1.call-done, f32[4,128,8192]{2,1,0:T(8,128)} %get-tuple-element.54, f32[4,128]{1,0:T(4,128)S(1)} %broadcast_maximum_fusion, f32[4,128]{1,0:T(4,128)S(1)} %fusion), kind=kOutput, calls=%fused_computation.26 | convolution fusion | flops 2193948672 | bytes 21368832 | tf_op jit(solution)/shard_map/htr,rhv->thv/dot_general | solution.py:159
  223.1 0.6 log_add_fusion
  223.8 1.0 multiply_add_fusion
  225.1 0.4 multiply_reduce_fusion.1
  226.0 49.8 %all-gather.8.cloned.1.call-done = bf16[1024,2048]{0,1:T(8,128)(2,1)} async-done(((bf16[1024,32]{0,1:T(8,128)(2,1)}), bf16[1024,2048]{0,1:T(8,128)(2,1)}) %all-gather.8.cloned.1.call-update) | async-done | bytes 4194320 | tf_op jit(solution)/shard_map/all_gather | solution.py:170
  275.9 3.7 %convolution_convert_fusion = bf16[128,2048]{1,0:T(8,128)(2,1)S(1)} fusion(bf16[1024,2048]{0,1:T(8,128)(2,1)} %all-gather.8.cloned.1.call-done, bf16[128,512]{1,0:T(8,128)(2,1)S(1)} %multiply_convert_fusion, bf16[128,512]{1,0:T(8,128)(2,1)S(1)} %copy.64), kind=kOutput, calls=%fused_computation.10 | convolution fusion | flops 537657344 | bytes 4980736 | tf_op jit(solution)/shard_map/dot_general | solution.py:168
  279.6 8.6 %all_to_all.5 = bf16[2,128,1024]{2,1,0:T(8,128)(2,1)S(1)} all-to-all(bf16[2,128,1024]{2,1,0:T(8,128)(2,1)S(1)} %bitcast.89), channel_id=1, replica_groups=mesh['sp'=64,'fs'=4,'tp'=2] {'tp'}, dimensions={0} | all-to-all | bytes 1048576 | tf_op jit(solution)/shard_map/all_to_all | solution.py:45
  288.2 0.8 reduce_sum.72
  (46 shorter events, 2.8 us)
Async XLA Ops:
  7.2 5.6 %copy-start = (bf16[2048,256]{1,0:T(8,128)(2,1)S(1)}, bf16[2048,256]{1,0:T(8,128)(2,1)}, u32[]{:S(2)}) copy-start(bf16[2048,256]{1,0:T(8,128)(2,1)} %param.20) | copy-start | bytes 3145732
  7.2 99.3 %all-gather.4.cloned.1.call-start = ((), (), s32[]{:S(2)}) async-start(), calls=%async_computation.1 | async-start | bytes 6389760 | tf_op jit(solution)/shard_map/all_gather | solution.py:21
  8.8 184.9 %all-gather.6.cloned.1.call-start = ((), (), s32[]{:S(2)}) async-start(), calls=%async_computation.2 | async-start | bytes 6340608 | tf_op jit(solution)/shard_map/all_gather | solution.py:130
  14.6 101.4 %copy-start.1 = (bf16[512,768]{1,0:T(8,128)(2,1)S(1)}, bf16[512,768]{1,0:T(8,128)(2,1)}, u32[]{:S(2)}) copy-start(bf16[512,768]{1,0:T(8,128)(2,1)} %param.23) | copy-start | bytes 2359300
  15.5 260.4 %all-gather.8.cloned.1.call-start = ((), (), s32[]{:S(2)}) async-start(), calls=%async_computation.3 | async-start | bytes 4259840 | tf_op jit(solution)/shard_map/all_gather | solution.py:170
  108.5 8.5 %copy-start.2 = (bf16[256,512]{1,0:T(8,128)(2,1)S(1)}, bf16[256,512]{1,0:T(8,128)(2,1)}, u32[]{:S(2)}) copy-start(bf16[256,512]{1,0:T(8,128)(2,1)} %param.24) | copy-start | bytes 786436
  110.6 113.2 %collective-permute-start = (bf16[15,512]{1,0:T(8,128)(2,1)S(1)}, bf16[15,512]{1,0:T(8,128)(2,1)S(1)}, u32[]{:S(2)}, u32[]{:S(2)}) collective-permute-start(bf16[15,512]{1,0:T(8,128)(2,1)S(1)} %get-tuple-element.8), channel_id=1, source_target_pairs={{0,8},{8,16},{16,24},{24,32},{32,40},{40,48},{48,56},{56,64},{64,7... | collective-permute-start | bytes 46088 | tf_op jit(solution)/shard_map/ppermute | solution.py:30
  112.6 111.3 %collective-permute-start.1 = (bf16[15,512]{1,0:T(8,128)(2,1)S(1)}, bf16[15,512]{1,0:T(8,128)(2,1)S(1)}, u32[]{:S(2)}, u32[]{:S(2)}) collective-permute-start(bf16[15,512]{1,0:T(8,128)(2,1)S(1)} %get-tuple-element.9), channel_id=1, source_target_pairs={{8,0},{16,8},{24,16},{32,24},{40,32},{48,40},{56,48},{64,56},{72,6... | collective-permute-start | bytes 46088 | tf_op jit(solution)/shard_map/ppermute | solution.py:33
Sparse Core Ops, SparseCore 0:
  11.6 94.8 all-gather.3
  109.6 84.0 all-gather.5
  196.7 79.1 all-gather.7
where the time goes:
time: 296 us
  waiting for transfers between devices  211 us (71%)
  matrix products  33.1 us (11%)
  other arithmetic  23.5 us (8%)
  between operations  14 us (5%)
  blocking collectives  8.59 us (3%)
  starting transfers between devices  3.33 us (1%)
    all_gather x1, waiting for transfers between devices, in_one_piece(): result = lax.all_gather(both, axis, axis=dim, tiled=True)  84.6 us
    all_gather x1, waiting for transfers between devices, per_device(): block_keys = lax.all_gather(own_keys, ('sp', 'tp'), axis=0, tiled=True)  76.4 us
    all_gather x1, waiting for transfers between devices, per_device(): lax.all_gather(out_weight, 'sp', axis=1, tiled=True)  49.8 us
    dot_general x1, matrix products, per_device(): jnp.einsum('hqc,kc->hqk', queries, block_keys, preferred_element_type=jnp...  10.9 us
    dot_general x1, matrix products, per_device(): jnp.einsum('htr,rhv->thv', attended, value_up.reshape(KVR, head_count, VD...  9.88 us
    reduce_sum x1, other arithmetic, per_device(): new_sum = jnp.sum(weights, axis=2)  8.7 us
    all_to_all x1, blocking collectives, sent_and_summed(): lax.all_to_all(tiles, axis, split_axis=0, concat_axis=0, tiled=True)  8.59 us
  transfers between devices with their start and end apart: 5, of which 3 were waited for; matrix products, arithmetic and copies ran while one was open for 18% of the time, Pallas kernels for 0%

commit v1 on v0

--- a/solution.py
+++ b/solution.py
@@ -127,7 +127,10 @@
     own_rows = lax.dynamic_slice_in_dim(normed, first_row, half_rows, 0)
     own_positions = lax.dynamic_slice_in_dim(offsets, first_row, half_rows, 0)
     own_keys = key_block(own_rows, latent_down, latent_gain, rope_down, own_positions)
-    block_keys = lax.all_gather(own_keys, ("sp", "tp"), axis=0, tiled=True)
+    block_keys = jnp.concatenate(
+        lax.all_to_all(jnp.stack([own_keys] * lax.axis_size(("sp", "tp"))), ("sp", "tp"), 0, 0),
+        axis=0,
+    )
     row_max = jnp.full((head_count, tok_count), far_below, jnp.float32)
     scores = (
         jnp.einsum("hqc,kc->hqk", queries, block_keys, preferred_element_type=jnp.float32)

time: 296 us -> 363 us (1.23)
  waiting for transfers between devices: 211 us -> 260 us
  starting transfers between devices: 3.33 us -> 22.2 us
  other arithmetic: 23.5 us -> 18.7 us
    all_gather x1, waiting for transfers between devices: 84.6 us -> 220 us  [in_one_piece(): result = lax.all_gather(both, axis, axis=dim, tiled=True)]
    all_gather x1 -> x0, waiting for transfers between devices: 76.4 us -> none  [per_device(): block_keys = lax.all_gather(own_keys, ('sp', 'tp'), axis=0, tiled=True)]
    all_to_all x0 -> x1, starting transfers between devices: none -> 19 us  [per_device(): lax.all_to_all(jnp.stack([own_keys] * lax.axis_size(('sp', 'tp'))), ('sp'...]
    all_gather x1, waiting for transfers between devices: 49.8 us -> 40.1 us  [per_device(): lax.all_gather(out_weight, 'sp', axis=1, tiled=True)]
    another operation x0 -> x1, local copies, waits for them, and re-layouts: none -> 3.69 us  [per_device(): jnp.stack([own_keys] * lax.axis_size(('sp', 'tp')))]
  transfers between devices with their start and end apart: 5 -> 5, of which waited for: 3 -> 2; matrix products, arithmetic and copies ran while one was open for 18% -> 14% of each run, Pallas kernels for 0% -> 0%
where the time goes in v1:
time: 363 us; the launch traced here: 362 us
  waiting for transfers between devices  260 us (72%)
  matrix products  33.3 us (9%)
  starting transfers between devices  22.2 us (6%)
  other arithmetic  18.7 us (5%)
  between operations  14.4 us (4%)
  blocking collectives  8.6 us (2%)
  local copies, waits for them, and re-layouts  4.97 us (1%)
    all_gather x1, waiting for transfers between devices, in_one_piece(): result = lax.all_gather(both, axis, axis=dim, tiled=True)  220 us
    all_gather x1, waiting for transfers between devices, per_device(): lax.all_gather(out_weight, 'sp', axis=1, tiled=True)  40.1 us
    all_to_all x1, starting transfers between devices, per_device(): lax.all_to_all(jnp.stack([own_keys] * lax.axis_size(('sp', 'tp'))), ('sp'...  19 us
    dot_general x1, matrix products, per_device(): jnp.einsum('hqc,kc->hqk', queries, block_keys, preferred_element_type=jnp...  11.1 us
    dot_general x1, matrix products, per_device(): jnp.einsum('htr,rhv->thv', attended, value_up.reshape(KVR, head_count, VD...  9.89 us
    reduce_sum x1, other arithmetic, per_device(): new_sum = jnp.sum(weights, axis=2)  8.65 us
    all_to_all x1, blocking collectives, sent_and_summed(): lax.all_to_all(tiles, axis, split_axis=0, concat_axis=0, tiled=True)  8.6 us
  transfers between devices with their start and end apart: 5, of which 2 were waited for; matrix products, arithmetic and copies ran while one was open for 14% of the time, Pallas kernels for 0%

profile of v1, /device:TPU:1, one launch (start us, length us, event | category | flops | bytes accessed | tf_op | source)
XLA Modules:
  0.0 362.1 jit_solution(17004816863158831909)
XLA Ops:
  7.2 1.5 pad_maximum_fusion.2
  8.8 0.7 convert_element_type.239
  9.4 0.7 convert_element_type.232
  10.2 1.2 fusion.30
  11.5 1.2 fusion.32
  12.7 0.4 multiply_reduce_fusion.3
  13.2 1.2 fusion.52
  14.4 0.2 subtract_convert_fusion.1
  14.8 3.7 %stack.2 = bf16[128,64,320]{2,1,0:T(8,128)(2,1)} broadcast(bf16[64,320]{1,0:T(8,128)(2,1)S(1)} %pad_maximum_fusion.4), dimensions={1,2} | broadcast | bytes 5283840 | tf_op jit(solution)/shard_map/stack | solution.py:131
  18.5 19.0 %all-to-all-start = ((bf16[128,64,320]{2,1,0:T(8,128)(2,1)}), bf16[128,64,320]{2,1,0:T(8,128)(2,1)}, u32[]{:S(2)}, u32[]{:S(2)}) async-start(bf16[128,64,320]{2,1,0:T(8,128)(2,1)} %stack.2), calls=%async_computation | async-start | bytes 12582912 | tf_op jit(solution)/shard_map/all_to_all | solution.py:131
  37.5 0.6 pad_maximum_fusion.3
  38.8 219.8 %all-gather.3.cloned.1.call-done = bf16[2048,1536]{1,0:T(8,128)(2,1)} async-done(((bf16[32,1536]{1,0:T(8,128)(2,1)}), bf16[2048,1536]{1,0:T(8,128)(2,1)}) %all-gather.3.cloned.1.call-update) | async-done | bytes 6291472 | tf_op jit(solution)/shard_map/all_gather | solution.py:21
  258.6 2.1 fusion.24
  260.7 2.1 fusion.27
  262.8 1.9 collective-permute-start
  264.7 1.3 collective-permute-start.1
  266.0 2.1 multiply_reduce_fusion.2
  268.2 0.5 fusion.56
  269.2 0.3 convolution_convert_fusion.1
  269.5 11.1 %multiply_reduce_fusion = (f32[4,128]{1,0:T(4,128)S(1)}, f32[4,128,8192]{2,1,0:T(8,128)}) fusion(bf16[8192,320,1]{1,0,2:T(8,128)(2,1)} %bitcast.3, bf16[4,128,64]{2,1,0:T(8,128)(2,1)S(1)} %maximum_bitcast_fusion, bf16[4,128,256]{2,1,0:T(8,128)(2,1)S(1)} %convolution_convert_fusion.1), kind=kOutput, calls=%fused_computation.1 | convolution fusion | flops 2693398016 | bytes 22349824 | tf_op jit(solution)/shard_map/hqc,kc->hqk/dot_general | solution.py:136
  280.6 8.6 %fusion = f32[4,128]{1,0:T(4,128)S(1)} fusion(f32[4,128,8192]{2,1,0:T(8,128)} %get-tuple-element.54, f32[4,128]{1,0:T(4,128)S(1)} %broadcast_maximum_fusion), kind=kLoop, calls=%fused_computation.2 | loop fusion | flops 12582400 | bytes 16781312 | tf_op jit(solution)/shard_map/reduce_sum | solution.py:141
  289.2 9.9 %convolution_convert_fusion.2 = bf16[4,128,128]{1,2,0:T(8,128)(2,1)S(1)} fusion(bf16[256,4,128]{0,2,1:T(8,128)(2,1)S(1)} %bitcast.93, bf16[8192,320]{1,0:T(8,128)(2,1)} %bitcast.2, f32[4,128,8192]{2,1,0:T(8,128)} %get-tuple-element.54, f32[4,128]{1,0:T(4,128)S(1)} %broadcast_maximum_fusion, f32[4,128]{1,0:T(4,128)S(1)} %fusion), kind=kOutput, calls=%fused_computation.24 | convolution fusion | flops 2193948672 | bytes 21368832 | tf_op jit(solution)/shard_map/htr,rhv->thv/dot_general | solution.py:162
  299.1 0.6 log_add_fusion
  299.8 1.0 multiply_add_fusion
  300.9 0.2 reduce_sum.70
  301.1 0.4 multiply_reduce_fusion.1
  301.5 0.2 mul.764
  301.7 0.2 sub.45
  302.0 40.1 %all-gather.5.cloned.1.call-done = bf16[1024,2048]{0,1:T(8,128)(2,1)} async-done(((bf16[1024,32]{0,1:T(8,128)(2,1)}), bf16[1024,2048]{0,1:T(8,128)(2,1)}) %all-gather.5.cloned.1.call-update) | async-done | bytes 4194320 | tf_op jit(solution)/shard_map/all_gather | solution.py:173
  342.1 3.7 %convolution_convert_fusion = bf16[128,2048]{1,0:T(8,128)(2,1)S(1)} fusion(bf16[1024,2048]{0,1:T(8,128)(2,1)} %all-gather.5.cloned.1.call-done, bf16[128,512]{1,0:T(8,128)(2,1)S(1)} %multiply_convert_fusion, bf16[128,512]{1,0:T(8,128)(2,1)S(1)} %copy.69), kind=kOutput, calls=%fused_computation.8 | convolution fusion | flops 537657344 | bytes 4980736 | tf_op jit(solution)/shard_map/dot_general | solution.py:171
  345.9 8.6 %all_to_all.10 = bf16[2,128,1024]{2,1,0:T(8,128)(2,1)S(1)} all-to-all(bf16[2,128,1024]{2,1,0:T(8,128)(2,1)S(1)} %bitcast.88), channel_id=1, replica_groups=mesh['sp'=64,'fs'=4,'tp'=2] {'tp'}, dimensions={0} | all-to-all | bytes 1048576 | tf_op jit(solution)/shard_map/all_to_all | solution.py:45
  354.5 0.8 reduce_sum.72
  (58 shorter events, 2.0 us)
Async XLA Ops:
  7.2 5.6 %copy-start = (bf16[2048,256]{1,0:T(8,128)(2,1)S(1)}, bf16[2048,256]{1,0:T(8,128)(2,1)}, u32[]{:S(2)}) copy-start(bf16[2048,256]{1,0:T(8,128)(2,1)} %param.20) | copy-start | bytes 3145732
  7.2 251.4 %all-gather.3.cloned.1.call-start = ((), (), s32[]{:S(2)}) async-start(), calls=%async_computation.2 | async-start | bytes 6389760 | tf_op jit(solution)/shard_map/all_gather | solution.py:21
  18.5 19.1 %copy-start.5 = (bf16[512,32]{0,1:T(8,128)(2,1)S(1)}, bf16[512,32]{0,1:T(8,128)(2,1)}, u32[]{:S(2)}) copy-start(bf16[512,32]{0,1:T(8,128)(2,1)} %param.31) | copy-start | bytes 98308
  18.5 19.1 %copy-start.6 = (bf16[512,32]{0,1:T(8,128)(2,1)S(1)}, bf16[512,32]{0,1:T(8,128)(2,1)}, u32[]{:S(2)}) copy-start(bf16[512,32]{0,1:T(8,128)(2,1)} %param.30) | copy-start | bytes 98308
  18.5 19.9 %copy-start.7 = (bf16[512]{0:T(512)(128)(2,1)S(1)}, bf16[512]{0:T(512)(128)(2,1)}, u32[]{:S(2)}) copy-start(bf16[512]{0:T(512)(128)(2,1)} %param.19) | copy-start | bytes 3076
  18.5 19.9 %copy-start.8 = (bf16[512]{0:T(512)(128)(2,1)S(1)}, bf16[512]{0:T(512)(128)(2,1)}, u32[]{:S(2)}) copy-start(bf16[512]{0:T(512)(128)(2,1)} %param.29) | copy-start | bytes 3076
  18.5 20.1 %copy-start.3 = (bf16[256,512]{1,0:T(8,128)(2,1)S(1)}, bf16[256,512]{1,0:T(8,128)(2,1)}, u32[]{:S(2)}) copy-start(bf16[256,512]{1,0:T(8,128)(2,1)} %param.25) | copy-start | bytes 786436
  18.5 20.3 %copy-start.4 = (bf16[31,512]{1,0:T(8,128)(2,1)S(1)}, bf16[31,512]{1,0:T(8,128)(2,1)}, u32[]{:S(2)}) copy-start(bf16[31,512]{1,0:T(8,128)(2,1)} %param.28) | copy-start | bytes 95236
  18.5 251.0 %all-to-all-start = ((bf16[128,64,320]{2,1,0:T(8,128)(2,1)}), bf16[128,64,320]{2,1,0:T(8,128)(2,1)}, u32[]{:S(2)}, u32[]{:S(2)}) async-start(bf16[128,64,320]{2,1,0:T(8,128)(2,1)} %stack.2), calls=%async_computation | async-start | bytes 12582912 | tf_op jit(solution)/shard_map/all_to_all | solution.py:131
  37.4 230.7 %copy-start.1 = (bf16[512,768]{1,0:T(8,128)(2,1)S(1)}, bf16[512,768]{1,0:T(8,128)(2,1)}, u32[]{:S(2)}) copy-start(bf16[512,768]{1,0:T(8,128)(2,1)} %param.23) | copy-start | bytes 2359300
  37.5 304.7 %all-gather.5.cloned.1.call-start = ((), (), s32[]{:S(2)}) async-start(), calls=%async_computation.3 | async-start | bytes 4259840 | tf_op jit(solution)/shard_map/all_gather | solution.py:173
  260.7 8.5 %copy-start.2 = (bf16[256,512]{1,0:T(8,128)(2,1)S(1)}, bf16[256,512]{1,0:T(8,128)(2,1)}, u32[]{:S(2)}) copy-start(bf16[256,512]{1,0:T(8,128)(2,1)} %param.24) | copy-start | bytes 786436
  262.8 37.0 %collective-permute-start = (bf16[15,512]{1,0:T(8,128)(2,1)S(1)}, bf16[15,512]{1,0:T(8,128)(2,1)S(1)}, u32[]{:S(2)}, u32[]{:S(2)}) collective-permute-start(bf16[15,512]{1,0:T(8,128)(2,1)S(1)} %get-tuple-element.8), channel_id=1, source_target_pairs={{0,8},{8,16},{16,24},{24,32},{32,40},{40,48},{48,56},{56,64},{64,7... | collective-permute-start | bytes 46088 | tf_op jit(solution)/shard_map/ppermute | solution.py:30
  264.7 35.1 %collective-permute-start.1 = (bf16[15,512]{1,0:T(8,128)(2,1)S(1)}, bf16[15,512]{1,0:T(8,128)(2,1)S(1)}, u32[]{:S(2)}, u32[]{:S(2)}) collective-permute-start(bf16[15,512]{1,0:T(8,128)(2,1)S(1)} %get-tuple-element.9), channel_id=1, source_target_pairs={{8,0},{16,8},{24,16},{32,24},{40,32},{48,40},{56,48},{64,56},{72,6... | collective-permute-start | bytes 46088 | tf_op jit(solution)/shard_map/ppermute | solution.py:33
Sparse Core Ops, SparseCore 0:
  11.6 246.9 all-gather.2
  261.7 80.4 all-gather.4
